TPU v7x, 32 devices: a whole 2x2x4 slice. The times are simulated.
32 devices in a mesh: sp: 8 (over z, x), tp: 4 (over y, core).
Axes of the slice: x: 2, y: 2, z: 4, core: 2. Of those that a mesh axis runs over, the one named last changes fastest.
Arguments:
- queries: bfloat16 [4096, 1024], P('sp', 'tp'), may hold values from -5.5 to 5.5
- key_vectors: bfloat16 [4096, 1024], P('sp', 'tp'), may hold values from -5.5 to 5.5
- latents: bfloat16 [4096, 2048], P('sp', 'tp'), may hold values from -6 to 6
- w_value: bfloat16 [2048, 1024], P(None, 'tp'), may hold values from -0.125 to 0.125
- log_sums: float32 [4096, 16], P('sp', 'tp'), as said below
- out_pair: bfloat16 [4096, 2048], P('sp', 'tp'), may hold values from -6 to 6
- cotangent: bfloat16 [4096, 1024], P('sp', 'tp'), may hold values from -6 to 6
- lambdas: float32 [8], P('tp'), may hold values from 0.3 to 0.8
- out_gain: float32 [128], replicated, may hold values from 0.1 to 1.9
Outputs:
- query_grad: float32 [4096, 1024], P('sp', 'tp')
- key_grad: float32 [4096, 1024], P('sp', 'tp')
- value_grad: float32 [4096, 1024], P('sp', 'tp')
- weight_grad: float32 [2048, 1024], P('sp', 'tp')
Inputs may be any that keep to these rules, and one draw needn't show every extreme that they name: `log_sums`: each entry is the logarithm of the sum of exp(scores_c[t, s]) over s <= t for its row t, head h and map c.
All inputs are finite; a program needn't handle non-finite values.
Results may differ from a plain program's by a relative error of at most 0.008.
Values may be sent and summed in bfloat16 or wider, within the bound.
A program may use at most 64 MiB of HBM per device.

v0:
```python
import jax
import jax.numpy as jnp
from jax import lax
from jax.sharding import PartitionSpec as P

norm_floor = 0.25
block_rows = 512


def head_cotangent(out_pair, cotangent, lambdas, out_gain):
    tok_rows = out_pair.shape[0]
    head_count = lambdas.shape[0]
    out_maps = out_pair.astype(jnp.float32).reshape(tok_rows, head_count, 2, -1)
    lam_cols = lambdas[None, :, None]
    merged = out_maps[:, :, 0] - lam_cols * out_maps[:, :, 1]
    inv_norm = lax.rsqrt(jnp.mean(merged * merged, axis=-1, keepdims=True) + norm_floor)
    scaled = cotangent.astype(jnp.float32).reshape(merged.shape) * out_gain
    inner_dot = jnp.mean(scaled * merged, axis=-1, keepdims=True)
    out_grad = (inv_norm * scaled - merged * (inv_norm * inv_norm * inv_norm) * inner_dot).astype(
        jnp.bfloat16
    )
    grad_wide = out_grad.astype(jnp.float32)
    first_map = jnp.sum(grad_wide * out_maps[:, :, 0], axis=-1)
    second_map = -lambdas[None, :] * jnp.sum(grad_wide * out_maps[:, :, 1], axis=-1)
    return (out_grad, jnp.stack([first_map, second_map], axis=-1))


def block_terms(
    query_block,
    key_block,
    value_block,
    grad_block,
    log_block,
    term_block,
    lambdas,
    query_pos,
    key_pos,
):
    factor = query_block.shape[-1] ** (-0.5)
    scores = (
        jnp.einsum("qhcd,khcd->hcqk", query_block, key_block, preferred_element_type=jnp.float32)
        * factor
    )
    visible = key_pos[None, :] <= query_pos[:, None]
    shifted = scores - jnp.transpose(log_block, (1, 2, 0))[..., None]
    softmax_maps = jnp.where(visible, jnp.exp(shifted), 0.0)
    value_dot = jnp.einsum(
        "qhe,khe->hqk", grad_block, value_block, preferred_element_type=jnp.float32
    )
    lam_cols = lambdas[:, None, None]
    weights = (softmax_maps[:, 0] - lam_cols * softmax_maps[:, 1]).astype(jnp.bfloat16)
    term_cols = jnp.transpose(term_block, (1, 2, 0))
    first_map = softmax_maps[:, 0] * (value_dot - term_cols[:, 0, :, None])
    second_map = softmax_maps[:, 1] * (-lam_cols * value_dot - term_cols[:, 1, :, None])
    dscore = (jnp.stack([first_map, second_map], axis=1) * factor).astype(jnp.bfloat16)
    return (weights, dscore)


def block_span():
    return block_rows


def per_device(
    queries, key_vectors, latents, w_value, log_sums, out_pair, cotangent, lambdas, out_gain
):
    tok_rows = queries.shape[0]
    head_count = lambdas.shape[0]
    offset = lax.axis_index("sp") * tok_rows
    own_pos = offset + jnp.arange(tok_rows, dtype=jnp.int32)
    last_pos = offset + tok_rows - 1
    gathered = lax.all_gather(latents, "tp", axis=1, tiled=True)
    values = jnp.dot(gathered, w_value, preferred_element_type=jnp.float32).astype(jnp.bfloat16)
    out_grad, row_terms = head_cotangent(out_pair, cotangent, lambdas, out_gain)
    query_heads = queries.reshape(tok_rows, head_count, 2, -1)
    key_heads = key_vectors.reshape(tok_rows, head_count, 2, -1)
    value_heads = values.reshape(tok_rows, head_count, -1)
    log_heads = log_sums.reshape(tok_rows, head_count, 2)
    grad_flat = out_grad.reshape(tok_rows, -1)
    term_flat = row_terms.reshape(tok_rows, -1)
    zero_keys = jnp.zeros(key_heads.shape, jnp.float32)
    zero_values = jnp.zeros(value_heads.shape, jnp.float32)
    shards = (
        lax.all_gather(key_vectors, "sp", axis=0, tiled=True),
        lax.all_gather(values, "sp", axis=0, tiled=True),
    )
    key_piece = shards[0]
    value_piece = shards[1]
    piece_rows = key_piece.shape[0]
    block_len = block_span()

    def query_add_block(block_idx, partial_value):
        begin_row = block_idx * block_len
        key_block = lax.dynamic_slice_in_dim(key_piece, begin_row, block_len, 0).reshape(
            block_len, head_count, 2, -1
        )
        value_block = lax.dynamic_slice_in_dim(value_piece, begin_row, block_len, 0).reshape(
            block_len, head_count, -1
        )
        key_pos = begin_row + jnp.arange(block_len, dtype=jnp.int32)

        def query_compute(sums):
            weights, dscore = block_terms(
                query_heads,
                key_block,
                value_block,
                out_grad,
                log_heads,
                row_terms,
                lambdas,
                own_pos,
                key_pos,
            )
            return sums + jnp.einsum(
                "hcqk,khcd->qhcd", dscore, key_block, preferred_element_type=jnp.float32
            )

        return lax.cond(begin_row <= last_pos, query_compute, lambda sums: sums, partial_value)

    query_grad = lax.fori_loop(0, piece_rows // block_len, query_add_block, zero_keys)
    shards = (
        lax.all_gather(queries.astype(jnp.float32), "sp", axis=0, tiled=True).astype(jnp.bfloat16),
        lax.all_gather(grad_flat.astype(jnp.float32), "sp", axis=0, tiled=True).astype(
            jnp.bfloat16
        ),
        lax.all_gather(log_sums, "sp", axis=0, tiled=True),
        lax.all_gather(term_flat, "sp", axis=0, tiled=True),
    )
    query_piece = shards[0]
    grad_piece = shards[1]
    log_piece = shards[2]
    term_piece = shards[3]
    piece_rows = query_piece.shape[0]
    key_block_len = block_span()

    def key_add_block(block_idx, partial_value):
        begin_row = block_idx * key_block_len
        query_block = lax.dynamic_slice_in_dim(query_piece, begin_row, key_block_len, 0).reshape(
            key_block_len, head_count, 2, -1
        )
        grad_block = lax.dynamic_slice_in_dim(grad_piece, begin_row, key_block_len, 0).reshape(
            key_block_len, head_count, -1
        )
        log_block = lax.dynamic_slice_in_dim(log_piece, begin_row, key_block_len, 0).reshape(
            key_block_len, head_count, 2
        )
        term_block = lax.dynamic_slice_in_dim(term_piece, begin_row, key_block_len, 0).reshape(
            key_block_len, head_count, 2
        )
        query_pos = begin_row + jnp.arange(key_block_len, dtype=jnp.int32)

        def key_compute(sums):
            weights, dscore = block_terms(
                query_block,
                key_heads,
                value_heads,
                grad_block,
                log_block,
                term_block,
                lambdas,
                query_pos,
                own_pos,
            )
            key_sum = sums[0] + jnp.einsum(
                "hcqk,qhcd->khcd", dscore, query_block, preferred_element_type=jnp.float32
            )
            value_sum = sums[1] + jnp.einsum(
                "hqk,qhe->khe", weights, grad_block, preferred_element_type=jnp.float32
            )
            return (key_sum, value_sum)

        return lax.cond(
            begin_row + key_block_len - 1 >= offset, key_compute, lambda sums: sums, partial_value
        )

    key_grad, value_grad = lax.fori_loop(
        0, piece_rows // key_block_len, key_add_block, (zero_keys, zero_values)
    )
    value_flat = value_grad.reshape(tok_rows, -1)
    value_narrow = value_flat.astype(jnp.bfloat16)
    weight_grad = lax.psum_scatter(
        lax.dot_general(
            gathered, value_narrow, (((0,), (0,)), ((), ())), preferred_element_type=jnp.float32
        ),
        "sp",
        scatter_dimension=0,
        tiled=True,
    )
    return (
        query_grad.reshape(tok_rows, -1),
        key_grad.reshape(tok_rows, -1),
        value_flat,
        weight_grad,
    )


def solution(mesh):
    return jax.shard_map(
        per_device,
        mesh=mesh,
        in_specs=(
            P("sp", "tp"),
            P("sp", "tp"),
            P("sp", "tp"),
            P(None, "tp"),
            P("sp", "tp"),
            P("sp", "tp"),
            P("sp", "tp"),
            P("tp"),
            P(),
        ),
        out_specs=(P("sp", "tp"), P("sp", "tp"), P("sp", "tp"), P("sp", "tp")),
        check_vma=False,
    )
```

profile of v0, /device:TPU:0, one launch (start us, length us, event | category | flops | bytes accessed | tf_op | source)
XLA Modules:
  0.0 320.5 jit_solution(6820730226512585887)
XLA Ops:
  8.0 1.8 copy.48
  9.9 1.3 copy.49
  12.9 1.8 copy.47
  14.8 20.2 %all-gather.8.cloned.1.call-done = bf16[512,2048]{1,0:T(8,128)(2,1)} async-done(((bf16[512,512]{1,0:T(8,128)(2,1)}), bf16[512,2048]{1,0:T(8,128)(2,1)}) %all-gather.8.cloned.1.call-update) | async-done | bytes 2097168 | tf_op jit(solution)/shard_map/all_gather | solution.py:71
  34.9 3.1 convolution_convert_fusion
  38.7 31.0 %all_gather.25 = f32[4096,4]{0,1:T(4,128)S(1)} all-gather(f32[512,4]{0,1:T(4,128)S(1)} %copy-done.6), channel_id=1, replica_groups=mesh['sp'=8,'tp'=4] {'sp'}, dimensions={0}, use_global_device_ids=true | all-gather | bytes 73728 | tf_op jit(solution)/shard_map/all_gather | solution.py:125
  69.7 31.9 %all_gather.27 = f32[4096,4]{0,1:T(4,128)} all-gather(f32[512,4]{0,1:T(4,128)S(1)} %reshape.188), channel_id=1, replica_groups=mesh['sp'=8,'tp'=4] {'sp'}, dimensions={0}, use_global_device_ids=true | all-gather | bytes 73728 | tf_op jit(solution)/shard_map/all_gather | solution.py:126
  102.8 37.0 %all-gather.14.cloned.1.call-done = bf16[4096,256]{0,1:T(8,128)(2,1)} async-done(((bf16[512,256]{0,1:T(8,128)(2,1)}), bf16[4096,256]{0,1:T(8,128)(2,1)}) %all-gather.14.cloned.1.call-update) | async-done | bytes 2097168 | tf_op jit(solution)/shard_map/all_gather | solution.py:122
  139.9 90.7 %while.39 = (s32[]{:T(128)}, f32[512,2,2,64]{0,3,2,1:T(8,128)S(1)}, f32[512,2,128]{2,0,1:T(8,128)S(1)}, s32[]{:T(128)}, bf16[4096,256]{0,1:T(8,128)(2,1)}, /*ind...) while((s32[]{:T(128)}, f32[512,2,2,64]{0,3,2,1:T(8,128)S(1)}, ...), condition=%wide.region_11.12_spmd.clone.clone, body=%wide.region_8.11_spmd.clone.clone.sunk | while | flops 547881984 | bytes 43121072 | solution.py:175
  140.0 11.3 %conditional.8 = ((f32[512,2,2,64]{0,3,2,1:T(8,128)S(1)}, f32[512,2,128]{2,0,1:T(8,128)S(1)})) conditional(s32[]{:T(128)} %convert_element_type.110, (f32[512,2,2,64]{0,3,2,1:T(8,128)S(1)}, f32[512,2,128]{2,0,1:T(8,128)S(1)}) %tuple.152, (s32[]{:T(128)}, s32[]{:T(128)}, s32[512]{0:T(512)S(1)}, bf16[4096,256]{0,1:T(8,128)(2,1)}, ...), branch_computations={%region_9.9_spmd, %region_10.10_spmd} | conditional | flops 547881984 | bytes 43118728 | solution.py:171
  142.0 3.2 exponential_select_fusion
  145.2 2.9 multiply_bitcast_fusion.1
  148.7 1.7 copy-done.1
  151.3 11.3 %conditional.8 = ((f32[512,2,2,64]{0,3,2,1:T(8,128)S(1)}, f32[512,2,128]{2,0,1:T(8,128)S(1)})) conditional(s32[]{:T(128)} %convert_element_type.110, (f32[512,2,2,64]{0,3,2,1:T(8,128)S(1)}, f32[512,2,128]{2,0,1:T(8,128)S(1)}) %tuple.152, (s32[]{:T(128)}, s32[]{:T(128)}, s32[512]{0:T(512)S(1)}, bf16[4096,256]{0,1:T(8,128)(2,1)}, ...), branch_computations={%region_9.9_spmd, %region_10.10_spmd} | conditional | flops 547881984 | bytes 43118728 | solution.py:171
  153.4 3.2 exponential_select_fusion
  156.6 2.9 multiply_bitcast_fusion.1
  160.1 1.7 copy-done.1
  162.6 11.4 %conditional.8 = ((f32[512,2,2,64]{0,3,2,1:T(8,128)S(1)}, f32[512,2,128]{2,0,1:T(8,128)S(1)})) conditional(s32[]{:T(128)} %convert_element_type.110, (f32[512,2,2,64]{0,3,2,1:T(8,128)S(1)}, f32[512,2,128]{2,0,1:T(8,128)S(1)}) %tuple.152, (s32[]{:T(128)}, s32[]{:T(128)}, s32[512]{0:T(512)S(1)}, bf16[4096,256]{0,1:T(8,128)(2,1)}, ...), branch_computations={%region_9.9_spmd, %region_10.10_spmd} | conditional | flops 547881984 | bytes 43118728 | solution.py:171
  164.7 3.2 exponential_select_fusion
  167.9 3.1 multiply_bitcast_fusion.1
  171.6 1.6 copy-done.1
  174.1 11.3 %conditional.8 = ((f32[512,2,2,64]{0,3,2,1:T(8,128)S(1)}, f32[512,2,128]{2,0,1:T(8,128)S(1)})) conditional(s32[]{:T(128)} %convert_element_type.110, (f32[512,2,2,64]{0,3,2,1:T(8,128)S(1)}, f32[512,2,128]{2,0,1:T(8,128)S(1)}) %tuple.152, (s32[]{:T(128)}, s32[]{:T(128)}, s32[512]{0:T(512)S(1)}, bf16[4096,256]{0,1:T(8,128)(2,1)}, ...), branch_computations={%region_9.9_spmd, %region_10.10_spmd} | conditional | flops 547881984 | bytes 43118728 | solution.py:171
  176.1 3.2 exponential_select_fusion
  179.4 2.9 multiply_bitcast_fusion.1
  182.9 1.7 copy-done.1
  185.4 11.2 %conditional.8 = ((f32[512,2,2,64]{0,3,2,1:T(8,128)S(1)}, f32[512,2,128]{2,0,1:T(8,128)S(1)})) conditional(s32[]{:T(128)} %convert_element_type.110, (f32[512,2,2,64]{0,3,2,1:T(8,128)S(1)}, f32[512,2,128]{2,0,1:T(8,128)S(1)}) %tuple.152, (s32[]{:T(128)}, s32[]{:T(128)}, s32[512]{0:T(512)S(1)}, bf16[4096,256]{0,1:T(8,128)(2,1)}, ...), branch_computations={%region_9.9_spmd, %region_10.10_spmd} | conditional | flops 547881984 | bytes 43118728 | solution.py:171
  187.4 3.2 exponential_select_fusion
  190.7 2.9 multiply_bitcast_fusion.1
  194.2 1.6 copy-done.1
  196.7 11.3 %conditional.8 = ((f32[512,2,2,64]{0,3,2,1:T(8,128)S(1)}, f32[512,2,128]{2,0,1:T(8,128)S(1)})) conditional(s32[]{:T(128)} %convert_element_type.110, (f32[512,2,2,64]{0,3,2,1:T(8,128)S(1)}, f32[512,2,128]{2,0,1:T(8,128)S(1)}) %tuple.152, (s32[]{:T(128)}, s32[]{:T(128)}, s32[512]{0:T(512)S(1)}, bf16[4096,256]{0,1:T(8,128)(2,1)}, ...), branch_computations={%region_9.9_spmd, %region_10.10_spmd} | conditional | flops 547881984 | bytes 43118728 | solution.py:171
  198.7 3.2 exponential_select_fusion
  202.0 2.9 multiply_bitcast_fusion.1
  205.5 1.7 copy-done.1
  208.0 11.2 %conditional.8 = ((f32[512,2,2,64]{0,3,2,1:T(8,128)S(1)}, f32[512,2,128]{2,0,1:T(8,128)S(1)})) conditional(s32[]{:T(128)} %convert_element_type.110, (f32[512,2,2,64]{0,3,2,1:T(8,128)S(1)}, f32[512,2,128]{2,0,1:T(8,128)S(1)}) %tuple.152, (s32[]{:T(128)}, s32[]{:T(128)}, s32[512]{0:T(512)S(1)}, bf16[4096,256]{0,1:T(8,128)(2,1)}, ...), branch_computations={%region_9.9_spmd, %region_10.10_spmd} | conditional | flops 547881984 | bytes 43118728 | solution.py:171
  210.1 3.2 exponential_select_fusion
  213.3 2.9 multiply_bitcast_fusion.1
  216.8 1.6 copy-done.1
  219.3 11.3 %conditional.8 = ((f32[512,2,2,64]{0,3,2,1:T(8,128)S(1)}, f32[512,2,128]{2,0,1:T(8,128)S(1)})) conditional(s32[]{:T(128)} %convert_element_type.110, (f32[512,2,2,64]{0,3,2,1:T(8,128)S(1)}, f32[512,2,128]{2,0,1:T(8,128)S(1)}) %tuple.152, (s32[]{:T(128)}, s32[]{:T(128)}, s32[512]{0:T(512)S(1)}, bf16[4096,256]{0,1:T(8,128)(2,1)}, ...), branch_computations={%region_9.9_spmd, %region_10.10_spmd} | conditional | flops 547881984 | bytes 43118728 | solution.py:171
  221.4 3.2 exponential_select_fusion
  224.6 3.0 multiply_bitcast_fusion.1
  228.1 1.7 copy-done.1
  230.7 3.9 %convolution_bitcast_fusion.1 = f32[2048,256]{0,1:T(8,128)} fusion(bf16[512,2048]{1,0:T(8,128)(2,1)} %all-gather.8.cloned.1.call-done, f32[512,256]{1,0:T(8,128)S(1)} %copy_bitcast_fusion.2), kind=kOutput, calls=%fused_computation.46 | convolution fusion | flops 537001984 | bytes 4718592 | tf_op jit(solution)/shard_map/dot_general | solution.py:181
  235.8 5.5 %all-gather.10.cloned.1.call-done = bf16[4096,256]{0,1:T(8,128)(2,1)} async-done(((bf16[512,256]{0,1:T(8,128)(2,1)}), bf16[4096,256]{0,1:T(8,128)(2,1)}) %all-gather.10.cloned.1.call-update) | async-done | bytes 2097168 | tf_op jit(solution)/shard_map/all_gather | solution.py:84
  241.4 4.3 %while.38 = (s32[]{:T(128)}, f32[512,2,2,64]{0,3,2,1:T(8,128)S(1)}, s32[]{:T(128)}, bf16[4096,256]{0,1:T(8,128)(2,1)}, bf16[512,2,2,64]{0,3,2,1:T(8,128)(2,1)S(1...) while((s32[]{:T(128)}, f32[512,2,2,64]{0,3,2,1:T(8,128)S(1)}, ...), condition=%wide.region_7.8_spmd.clone, body=%wide.region_4.7_spmd.clone.sunk | while | flops 411960320 | bytes 20756812 | solution.py:119
  241.4 3.9 %conditional.7 = (f32[512,2,2,64]{0,3,2,1:T(8,128)S(1)}) conditional(s32[]{:T(128)} %convert_element_type.109, f32[512,2,2,64]{0,3,2,1:T(8,128)S(1)} %get-tuple-element.1245, (s32[]{:T(128)}, s32[512]{0:T(512)S(1)}, s32[]{:T(128)}, bf16[4096,256]{0,1:T(8,128)(2,1)}, bf16[512,2,2,64]{0,3,2,1:T(8,128)(2,1)S(1)}, /*index=5*/f32[512,2,2]{0,2,1:T(2,128)S(1)}, ...), branch_computations={%region_5.0_spmd, %region_6.6_spmd} | conditional | flops 411960320 | bytes 20754510 | solution.py:117
  242.7 1.3 bitcast_select_fusion
  246.7 65.2 %reduce-scatter.2.cloned.1.call-done = f32[256,256]{0,1:T(8,128)} async-done(((f32[2048,256]{0,1:T(8,128)}), f32[256,256]{0,1:T(8,128)}) %reduce-scatter.2.cloned.1.call-update) | async-done | bytes 262160 | tf_op jit(solution)/shard_map/reduce_scatter | solution.py:180
  311.8 1.8 copy.60
  (186 shorter events, 36.7 us)
Async XLA Ops:
  7.2 27.7 %copy-start = (bf16[2048,256]{1,0:T(8,128)(2,1)S(1)}, bf16[2048,256]{1,0:T(8,128)(2,1)}, u32[]{:S(2)}) copy-start(bf16[2048,256]{1,0:T(8,128)(2,1)} %param.20) | copy-start | bytes 3145732
  7.2 3.9 %copy-start.5 = (bf16[512,256]{1,0:T(8,128)(2,1)S(1)}, bf16[512,256]{1,0:T(8,128)(2,1)}, u32[]{:S(2)}) copy-start(bf16[512,256]{1,0:T(8,128)(2,1)} %param.23) | copy-start | bytes 786436
  7.2 4.1 %copy-start.8 = (f32[128]{0:T(128)S(1)}, f32[128]{0:T(128)}, u32[]{:S(2)}) copy-start(f32[128]{0:T(128)} %param.25) | copy-start | bytes 1540
  7.2 4.1 %copy-start.7 = (f32[2]{0:T(128)S(1)}, f32[2]{0:T(128)}, u32[]{:S(2)}) copy-start(f32[2]{0:T(128)} %param.24) | copy-start | bytes 28
  7.2 27.7 %all-gather.8.cloned.1.call-start = ((), (), s32[]{:S(2)}) async-start(), calls=%async_computation.2 | async-start | bytes 2621440 | tf_op jit(solution)/shard_map/all_gather | solution.py:71
  7.9 94.8 %all-gather.12.cloned.1.call-start = ((), (), s32[]{:S(2)}) async-start(), calls=%async_computation.4 | async-start | bytes 2359296 | tf_op jit(solution)/shard_map/all_gather | solution.py:121
  9.8 130.0 %all-gather.14.cloned.1.call-start = ((), (), s32[]{:S(2)}) async-start(), calls=%async_computation.5 | async-start | bytes 2359296 | tf_op jit(solution)/shard_map/all_gather | solution.py:122
  12.8 222.9 %all-gather.6.cloned.1.call-start = ((), (), s32[]{:S(2)}) async-start(), calls=%async_computation.1 | async-start | bytes 2359296 | tf_op jit(solution)/shard_map/all_gather | solution.py:83
  14.7 226.6 %all-gather.10.cloned.1.call-start = ((), (), s32[]{:S(2)}) async-start(), calls=%async_computation.3 | async-start | bytes 2359296 | tf_op jit(solution)/shard_map/all_gather | solution.py:84
  38.0 0.7 copy-start.6
  38.0 101.9 %copy-start.4 = (bf16[512,256]{0,1:T(8,128)(2,1)S(1)}, bf16[512,256]{0,1:T(8,128)(2,1)}, u32[]{:S(2)}) copy-start(bf16[512,256]{0,1:T(8,128)(2,1)} %copy.47) | copy-start | bytes 786436
  38.0 273.8 %reduce-scatter.2.cloned.1.call-start = ((), (), s32[]{:S(2)}) async-start(), calls=%async_computation.6 | async-start | bytes 2359296 | tf_op jit(solution)/shard_map/reduce_scatter | solution.py:180
  148.2 2.3 copy-start.1
  159.6 2.2 copy-start.1
  171.0 2.2 copy-start.1
  182.3 2.2 copy-start.1
  193.6 2.2 copy-start.1
  204.9 2.2 copy-start.1
  216.2 2.2 copy-start.1
  227.6 2.2 copy-start.1
  230.7 3.9 %copy-start.2 = (f32[512,256]{1,0:T(8,128)}, f32[512,256]{1,0:T(8,128)S(1)}, u32[]{:S(2)}) copy-start(f32[512,256]{1,0:T(8,128)S(1)} %copy_bitcast_fusion.2) | copy-start | bytes 1572868
  234.6 6.8 %copy-start.3 = (bf16[512,256]{0,1:T(8,128)(2,1)S(1)}, bf16[512,256]{0,1:T(8,128)(2,1)}, u32[]{:S(2)}) copy-start(bf16[512,256]{0,1:T(8,128)(2,1)} %copy.48) | copy-start | bytes 786436
Sparse Core Ops, SparseCore 0:
  9.6 25.2 all-gather.7
  37.5 50.9 all-gather.11
  91.1 48.6 all-gather.13
  142.3 48.5 all-gather.5
  192.7 48.5 all-gather.9
  244.7 67.0 reduce-scatter.1
where the time goes:
time: 322 us; the launch traced here: 320 us
  waiting for transfers between devices  129 us (40%)
  matrix products  69.3 us (22%)
  blocking collectives  62.9 us (20%)
  local copies, waits for them, and re-layouts  39.8 us (12%)
  between operations  14.3 us (4%)
  other arithmetic  3.63 us (1%)
    reduce_scatter x1, waiting for transfers between devices, per_device(): lax.psum_scatter(lax.dot_general(gathered, value_narrow, (((0,), (0,)), (...  65.2 us
    all_gather x1, waiting for transfers between devices, per_device(): lax.all_gather(grad_flat.astype(jnp.float32), 'sp', axis=0, tiled=True)  37 us
    all_gather x1, blocking collectives, per_device(): lax.all_gather(term_flat, 'sp', axis=0, tiled=True)  31.9 us
    all_gather x1, blocking collectives, per_device(): lax.all_gather(log_sums, 'sp', axis=0, tiled=True)  31 us
    dot_general x9, matrix products, block_terms(): jnp.einsum('qhcd,khcd->hcqk', query_block, key_block, preferred_element_t...  26.6 us
    dot_general x9, matrix products, block_terms(): jnp.einsum('qhe,khe->hqk', grad_block, value_block, preferred_element_typ...  24.4 us
    all_gather x1, waiting for transfers between devices, per_device(): gathered = lax.all_gather(latents, 'tp', axis=1, tiled=True)  20.2 us
    cond x32, local copies, waits for them, and re-layouts  13.3 us
  transfers between devices with their start and end apart: 6, of which 4 were waited for; matrix products, arithmetic and copies ran while one was open for 30% of the time, Pallas kernels for 0%

commit v1 on v0

v1 whole, which is shorter than its diff:
```python
import functools
import math

import jax
import jax.numpy as jnp
from jax import lax
from jax.experimental import pallas as pl
from jax.experimental.pallas import tpu as pltpu
from jax.sharding import PartitionSpec as P

MESH = pl.DeviceIdType.MESH
F32 = jnp.float32
BF16 = jnp.bfloat16
LOG2E = math.log2(math.e)
norm_floor = 0.25
TILE = 256


def dot_nn(a, b):
    return lax.dot_general(a, b, (((1,), (0,)), ((), ())), preferred_element_type=F32)


def dot_nt(a, b):
    return lax.dot_general(a, b, (((1,), (1,)), ((), ())), preferred_element_type=F32)


def dot_tn(a, b):
    return lax.dot_general(a, b, (((0,), (0,)), ((), ())), preferred_element_type=F32)


def halves(block, factor):
    width = block.shape[-1]
    lane = lax.broadcasted_iota(jnp.int32, block.shape, 1)
    wide = block.astype(F32) * factor
    return (
        jnp.where(lane < width // 2, wide, 0.0).astype(BF16),
        jnp.where(lane < width // 2, 0.0, wide).astype(BF16),
    )


def kernel(
    n,
    tp_n,
    q_ref,
    k_ref,
    lat_ref,
    w_ref,
    log_ref,
    pair_ref,
    cot_ref,
    lam_ref,
    gain_ref,
    dq_ref,
    dk_ref,
    dv_ref,
    dw_ref,
    kbuf,
    vbuf,
    qbuf,
    gbuf,
    abuf,
    lbuf,
    own_v,
    own_g,
    own_a,
    col_a,
    own_k2,
    own_q2,
    part,
    wbuf,
    lat_send,
    lat_recv,
    fwd_send,
    fwd_recv,
    k_send,
    k_recv,
    v_send,
    v_recv,
    q_send,
    q_recv,
    g_send,
    g_recv,
    a_send,
    a_recv,
    w_send,
    w_recv,
):
    heads = lam_ref.shape[0]
    rows = q_ref.shape[0]
    width = q_ref.shape[1] // heads
    me = lax.axis_index("sp")
    tp = lax.axis_index("tp")
    chain = n // 2
    pos = me // 2
    col = me % 2
    factor = (width // 2) ** (-0.5)

    barrier = pltpu.get_barrier_semaphore()

    def greet_sp(i, carry):
        @pl.when(i != me)
        def _():
            pl.semaphore_signal(barrier, inc=1, device_id=(i, tp), device_id_type=MESH)

        return carry

    def greet_tp(i, carry):
        @pl.when(i != tp)
        def _():
            pl.semaphore_signal(barrier, inc=1, device_id=(me, i), device_id_type=MESH)

        return carry

    lax.fori_loop(0, n, greet_sp, 0)
    lax.fori_loop(0, tp_n, greet_tp, 0)
    pl.semaphore_wait(barrier, n - 1 + tp_n - 1)

    core = tp % 2
    pair = tp // 2
    mate = 2 * pair + 1 - core
    pairs = tp_n // 2

    def rc(src, dst, ssem, rsem, dev):
        return pltpu.make_async_remote_copy(
            src_ref=src,
            dst_ref=dst,
            send_sem=ssem,
            recv_sem=rsem,
            device_id=dev,
            device_id_type=MESH,
        )

    def lat_copy(slot_src, y):
        return rc(
            lat_ref, lbuf.at[slot_src], lat_send.at[y], lat_recv.at[slot_src], (me, 2 * y + core)
        )

    def lat_mate():
        return rc(lat_ref, lbuf.at[tp], fwd_send.at[tp], fwd_recv.at[tp], (me, mate))

    def lat_fwd(src):
        return rc(lbuf.at[src], lbuf.at[src], fwd_send.at[src], fwd_recv.at[src], (me, mate))

    class Stream:
        def __init__(self, own, buf, ssem, rsem, step):
            self.own, self.buf, self.ssem, self.rsem, self.step = own, buf, ssem, rsem, step

        def onward(self):
            nxt = pos + self.step
            return jnp.logical_and(nxt >= 0, nxt < chain)

        def copies(self, src, ref):
            far = rc(
                ref,
                self.buf.at[src],
                self.ssem.at[0, src],
                self.rsem.at[src],
                (jnp.clip(me + 2 * self.step, 0, n - 1), tp),
            )
            side = rc(
                ref,
                self.buf.at[src],
                self.ssem.at[1, src],
                self.rsem.at[src],
                (2 * pos + 1 - col, tp),
            )
            return far, side

        def send_own(self, act):
            far, side = self.copies(me, self.own)

            @pl.when(self.onward())
            def _():
                getattr(far, act)()

            @pl.when(col == (0 if self.step == 1 else 1))
            def _():
                getattr(side, act)()

        def forward(self, src, act):
            far, side = self.copies(src, self.buf.at[src])
            getattr(side, act)()

            @pl.when(self.onward())
            def _():
                getattr(far, act)()

        def wait(self, src):
            self.copies(src, self.buf.at[src])[0].wait_recv()

    ks = Stream(k_ref, kbuf, k_send, k_recv, 1)
    vs = Stream(own_v, vbuf, v_send, v_recv, 1)
    qs = Stream(q_ref, qbuf, q_send, q_recv, -1)
    gs = Stream(own_g, gbuf, g_send, g_recv, -1)
    as_ = Stream(own_a, abuf, a_send, a_recv, -1)

    for y in range(pairs):

        @pl.when(y != pair)
        def _():
            lat_copy(tp, y).start()

    lat_mate().start()
    qs.send_own("start")
    ks.send_own("start")

    lane = lax.broadcasted_iota(jnp.int32, (rows, 128), 1)
    packed = jnp.zeros((rows, 128), F32)
    for h in range(heads):
        lam = lam_ref[h]
        a = pair_ref[:, (2 * h) * width : (2 * h + 1) * width].astype(F32)
        b = pair_ref[:, (2 * h + 1) * width : (2 * h + 2) * width].astype(F32)
        merged = a - lam * b
        inv = lax.rsqrt(jnp.mean(merged * merged, axis=-1, keepdims=True) + norm_floor)
        g = cot_ref[:, h * width : (h + 1) * width].astype(F32) * gain_ref[...]
        inner = jnp.mean(g * merged, axis=-1, keepdims=True)
        og = (inv * g - merged * (inv * inv * inv) * inner).astype(BF16)
        own_g[:, h * width : (h + 1) * width] = og
        wide = og.astype(F32)
        first = jnp.sum(wide * a, axis=-1, keepdims=True)
        second = jnp.sum(wide * b, axis=-1, keepdims=True)
        log_lam = jnp.log(jnp.full((1, 128), lam, F32))
        log0 = log_ref[:, 2 * h : 2 * h + 1] * LOG2E
        log1 = (log_ref[:, 2 * h + 1 : 2 * h + 2] - log_lam) * LOG2E
        packed = jnp.where(lane == 4 * h, log0, packed)
        packed = jnp.where(lane == 4 * h + 1, log1, packed)
        packed = jnp.where(lane == 4 * h + 2, first, packed)
        packed = jnp.where(lane == 4 * h + 3, second, packed)
    col_a[...] = packed
    own_a[...] = jnp.transpose(packed)[:8, :]
    gs.send_own("start")
    as_.send_own("start")

    for h in range(heads):
        sl = slice(h * width, (h + 1) * width)
        k0, k1 = halves(k_ref[:, sl], factor)
        own_k2[0, :, sl] = k0
        own_k2[1, :, sl] = k1
        q0, q1 = halves(q_ref[:, sl], factor)
        own_q2[0, :, sl] = q0
        own_q2[1, :, sl] = q1

    for y in range(pairs):

        @pl.when(y != pair)
        def _():
            src = 2 * y + core
            lat_copy(src, y).wait_recv()
            lat_fwd(src).start()

    local = w_ref.shape[0] // tp_n
    lat_own = pl.ds(pl.multiple_of(tp * local, local), local)
    dv_ref[...] = dot_nn(lat_ref[...], w_ref[lat_own, :])

    for y in range(pairs):
        other = 2 * y + 1 - core
        lat_fwd(other).wait_recv()

    def add_values(i, carry):
        @pl.when(i != tp)
        def _():
            dv_ref[...] += dot_nn(
                lbuf[i], w_ref[pl.ds(pl.multiple_of(i * local, local), local), :]
            )

        return carry

    lax.fori_loop(0, tp_n, add_values, 0)
    own_v[...] = dv_ref[...].astype(BF16)
    vs.send_own("start")

    def key_side(q_of, g_of, a_of, diagonal):
        for h in range(heads):
            sl = slice(h * width, (h + 1) * width)

            def tile(i, carry):
                ts = pl.ds(pl.multiple_of(i * TILE, TILE), TILE)
                q = q_of(sl)
                g = g_of(sl)
                q0, q1 = halves(q, factor)
                s0 = dot_nt(own_k2[0, ts, sl], q)
                s1 = dot_nt(own_k2[1, ts, sl], q)
                vd = dot_nt(own_v[ts, sl], g)
                p0 = jnp.exp2(s0 * LOG2E - a_of(4 * h))
                p1 = jnp.exp2(s1 * LOG2E - a_of(4 * h + 1))
                if diagonal:
                    spos = i * TILE + lax.broadcasted_iota(jnp.int32, (TILE, rows), 0)
                    tpos = lax.broadcasted_iota(jnp.int32, (TILE, rows), 1)
                    vis = spos <= tpos
                    p0 = jnp.where(vis, p0, 0.0)
                    p1 = jnp.where(vis, p1, 0.0)
                mixed = (p0 - p1).astype(BF16)
                d0 = (p0 * (vd - a_of(4 * h + 2))).astype(BF16)
                d1 = (p1 * (a_of(4 * h + 3) - vd)).astype(BF16)
                dvt = dot_nn(mixed, g)
                dkt = dot_nn(d0, q0) + dot_nn(d1, q1)
                if diagonal:
                    dv_ref[ts, sl] = dvt
                    dk_ref[ts, sl] = dkt
                else:
                    dv_ref[ts, sl] += dvt
                    dk_ref[ts, sl] += dkt
                return carry

            lax.fori_loop(0, rows // TILE, tile, 0)

    def query_side(k_of, v_of, diagonal):
        for h in range(heads):
            sl = slice(h * width, (h + 1) * width)

            def tile(i, carry):
                ts = pl.ds(pl.multiple_of(i * TILE, TILE), TILE)
                k = k_of(sl)
                v = v_of(sl)
                k0, k1 = halves(k, factor)
                s0 = dot_nt(own_q2[0, ts, sl], k)
                s1 = dot_nt(own_q2[1, ts, sl], k)
                vd = dot_nt(own_g[ts, sl], v)
                aux = col_a[ts, :]
                p0 = jnp.exp2(s0 * LOG2E - aux[:, 4 * h : 4 * h + 1])
                p1 = jnp.exp2(s1 * LOG2E - aux[:, 4 * h + 1 : 4 * h + 2])
                if diagonal:
                    tpos = i * TILE + lax.broadcasted_iota(jnp.int32, (TILE, rows), 0)
                    spos = lax.broadcasted_iota(jnp.int32, (TILE, rows), 1)
                    vis = spos <= tpos
                    p0 = jnp.where(vis, p0, 0.0)
                    p1 = jnp.where(vis, p1, 0.0)
                d0 = (p0 * (vd - aux[:, 4 * h + 2 : 4 * h + 3])).astype(BF16)
                d1 = (p1 * (aux[:, 4 * h + 3 : 4 * h + 4] - vd)).astype(BF16)
                dqt = dot_nn(d0, k0) + dot_nn(d1, k1)
                if diagonal:
                    dq_ref[ts, sl] = dqt
                else:
                    dq_ref[ts, sl] += dqt
                return carry

            lax.fori_loop(0, rows // TILE, tile, 0)

    key_side(
        lambda sl: q_ref[:, sl], lambda sl: own_g[:, sl], lambda r: own_a[r : r + 1, :], True
    )
    query_side(lambda sl: k_ref[:, sl], lambda sl: own_v[:, sl], True)

    def key_slot(src):
        key_side(
            lambda sl: qbuf[src, :, sl],
            lambda sl: gbuf[src, :, sl],
            lambda r: abuf[src, r : r + 1, :],
            False,
        )

    def query_slot(src):
        query_side(lambda sl: kbuf[src, :, sl], lambda sl: vbuf[src, :, sl], False)

    def step(s, carry):
        up_own = pos - (s + 1)
        down_own = pos + (s + 1)
        up_src = 2 * up_own + col
        down_src = 2 * down_own + col
        has_up = up_own >= 0
        has_down = down_own < chain
        up_side = 2 * (pos - s) + 1 - col
        down_side = 2 * (pos + s) + 1 - col
        side_up = jnp.logical_and(pos - s >= 0, jnp.logical_or(s > 0, col == 1))
        side_down = jnp.logical_and(pos + s < chain, jnp.logical_or(s > 0, col == 0))

        @pl.when(has_down)
        def _():
            for stream in (qs, gs, as_):
                stream.wait(down_src)
                stream.forward(down_src, "start")

        @pl.when(has_up)
        def _():
            ks.wait(up_src)
            ks.forward(up_src, "start")

        @pl.when(side_down)
        def _():
            for stream in (qs, gs, as_):
                stream.wait(down_side)
            key_slot(down_side)

        @pl.when(has_up)
        def _():
            vs.wait(up_src)
            vs.forward(up_src, "start")

        @pl.when(has_down)
        def _():
            key_slot(down_src)

        @pl.when(side_up)
        def _():
            ks.wait(up_side)
            vs.wait(up_side)
            query_slot(up_side)

        @pl.when(has_up)
        def _():
            query_slot(up_src)

        return carry

    lax.fori_loop(0, chain, step, 0)

    narrow = dv_ref[...].astype(BF16)
    part[pl.ds(pl.multiple_of(tp * local, local), local), :] = dot_tn(
        lat_ref[...], narrow
    ).astype(BF16)

    def add_part(i, carry):
        @pl.when(i != tp)
        def _():
            part[pl.ds(pl.multiple_of(i * local, local), local), :] = dot_tn(
                lbuf[i], dv_ref[...].astype(BF16)
            ).astype(BF16)

        return carry

    lax.fori_loop(0, tp_n, add_part, 0)

    block = dw_ref.shape[0]

    def w_copy(dst):
        return rc(
            part.at[pl.ds(pl.multiple_of(dst * block, block), block)],
            wbuf.at[me],
            w_send.at[dst],
            w_recv.at[me],
            (dst, tp),
        )

    def w_wait(src):
        rc(
            part.at[pl.ds(0, block)], wbuf.at[src], w_send.at[src], w_recv.at[src], (src, tp)
        ).wait_recv()

    def w_start(i, carry):
        w_copy((me + i) % n).start()
        return carry

    lax.fori_loop(1, n, w_start, 0)
    dw_ref[...] = part[pl.ds(pl.multiple_of(me * block, block), block), :].astype(F32)

    def w_add(i, carry):
        src = (me + n - i) % n
        w_wait(src)
        dw_ref[...] += wbuf[src].astype(F32)
        return carry

    lax.fori_loop(1, n, w_add, 0)

    def w_done(i, carry):
        w_copy((me + i) % n).wait_send()
        return carry

    lax.fori_loop(1, n, w_done, 0)

    for stream in (qs, ks, gs, as_, vs):
        stream.send_own("wait_send")

    def drain(s, carry):
        @pl.when(pos + s < chain)
        def _():
            for stream in (qs, gs, as_):
                stream.forward(2 * (pos + s) + col, "wait_send")

        @pl.when(pos - s >= 0)
        def _():
            for stream in (ks, vs):
                stream.forward(2 * (pos - s) + col, "wait_send")

        return carry

    lax.fori_loop(1, chain, drain, 0)
    lat_mate().wait_send()
    for y in range(pairs):

        @pl.when(y != pair)
        def _():
            lat_copy(tp, y).wait_send()
            lat_fwd(2 * y + core).wait_send()


def solution(mesh):
    n = mesh.shape["sp"]
    tp_n = mesh.shape["tp"]

    def step(q, k, lat, w, logs, pair, cot, lam, gain):
        rows, qcols = q.shape
        dmodel, vcols = w.shape
        block = dmodel // n
        vmem = pl.BlockSpec(memory_space=pltpu.VMEM)
        dma = pltpu.SemaphoreType.DMA
        return pl.pallas_call(
            functools.partial(kernel, n, tp_n),
            name="diff_backward",
            out_shape=(
                jax.ShapeDtypeStruct((rows, qcols), F32),
                jax.ShapeDtypeStruct((rows, qcols), F32),
                jax.ShapeDtypeStruct((rows, vcols), F32),
                jax.ShapeDtypeStruct((block, vcols), F32),
            ),
            in_specs=[vmem] * 7 + [pl.BlockSpec(memory_space=pltpu.SMEM), vmem],
            out_specs=(vmem,) * 4,
            scratch_shapes=[
                pltpu.VMEM((n, rows, qcols), BF16),
                pltpu.VMEM((n, rows, vcols), BF16),
                pltpu.VMEM((n, rows, qcols), BF16),
                pltpu.VMEM((n, rows, vcols), BF16),
                pltpu.VMEM((n, 8, rows), F32),
                pltpu.VMEM((tp_n,) + lat.shape, BF16),
                pltpu.VMEM((rows, vcols), BF16),
                pltpu.VMEM((rows, vcols), BF16),
                pltpu.VMEM((8, rows), F32),
                pltpu.VMEM((rows, 128), F32),
                pltpu.VMEM((2, rows, qcols), BF16),
                pltpu.VMEM((2, rows, qcols), BF16),
                pltpu.VMEM((dmodel, vcols), BF16),
                pltpu.VMEM((n, block, vcols), BF16),
                dma((tp_n // 2,)),
                dma((tp_n,)),
                dma((tp_n,)),
                dma((tp_n,)),
                dma((2, n)),
                dma((n,)),
                dma((2, n)),
                dma((n,)),
                dma((2, n)),
                dma((n,)),
                dma((2, n)),
                dma((n,)),
                dma((2, n)),
                dma((n,)),
                dma((n,)),
                dma((n,)),
            ],
            compiler_params=pltpu.CompilerParams(
                collective_id=0, has_side_effects=True, vmem_limit_bytes=60 * 1024 * 1024
            ),
        )(q, k, lat, w, logs, pair, cot, lam, gain.reshape(1, -1))

    return jax.shard_map(
        step,
        mesh=mesh,
        in_specs=(
            P("sp", "tp"),
            P("sp", "tp"),
            P("sp", "tp"),
            P(None, "tp"),
            P("sp", "tp"),
            P("sp", "tp"),
            P("sp", "tp"),
            P("tp"),
            P(),
        ),
        out_specs=(P("sp", "tp"), P("sp", "tp"), P("sp", "tp"), P("sp", "tp")),
        check_vma=False,
    )
```

time: 322 us -> 100 us (0.31)
  the two profiles are of different devices: /device:TPU:0 before, /device:TPU:27 now
where the time goes in v1:
time: 100 us
  Pallas kernels  93 us (93%)
  local copies, waits for them, and re-layouts  6.5 us (6%)
    pallas_call x1, Pallas kernels, step(): pl.pallas_call(functools.partial(kernel, n, tp_n), name='diff_backward',...  93 us
    unnamed x11, local copies, waits for them, and re-layouts  6.5 us

profile of v1, /device:TPU:27, one launch (start us, length us, event | category | flops | bytes accessed | tf_op | source)
XLA Modules:
  0.0 100.1 jit_solution(5756020127568554329)
XLA Ops:
  0.6 1.6 %copy.13.log_ref = f32[512,4]{1,0:T(8,128)} copy(f32[512,4]{0,1:T(4,128)} %param.13) | data formatting | bytes 16384 | tf_op args[4]
  2.2 93.0 %diff_backward.1 = (f32[512,256]{1,0:T(8,128)}, f32[512,256]{1,0:T(8,128)}, f32[512,256]{1,0:T(8,128)}, f32[256,256]{1,0:T(8,128)}) custom-call(bf16[512,256]{1,0:T(8,128)(2,1)} %q_ref.1, bf16[512,256]{1,0:T(8,128)(2,1)} %k_ref.1, bf16[512,512]{1,0:T(8,128)(2,1)} %lat_ref.1, bf16[2048,256]{1,0:T(8,128)(2,1)} %w_ref.1, f32[512,4]{1,0:T(8,128)} %copy.13.log_ref, ...), custom_call_target="tpu_custom_call" | custom-call | tf_op jit(solution)/shard_map/diff_backward/pallas_call | solution.py:496
  95.2 0.0 copy-start.1
  95.2 1.9 %copy.18 = f32[512,256]{1,0:T(8,128)} copy(f32[512,256]{1,0:T(8,128)} %get-tuple-element.8) | data formatting | bytes 1048576
  97.1 0.0 copy-done.1
  97.1 0.0 copy-start
  97.1 0.8 copy.19
  97.9 0.4 copy-done
  98.3 0.0 copy-start.2
  98.3 0.8 copy.20
  99.1 0.3 copy-done.2
  99.4 0.7 copy.21
Async XLA Ops:
  95.2 1.9 %copy-start.1 = (f32[512,256]{1,0:T(8,128)S(1)}, f32[512,256]{1,0:T(8,128)}, u32[]{:S(2)}) copy-start(f32[512,256]{1,0:T(8,128)} %get-tuple-element.9) | copy-start | bytes 1572868
  97.1 1.2 %copy-start = (f32[512,256]{1,0:T(8,128)S(1)}, f32[512,256]{1,0:T(8,128)}, u32[]{:S(2)}) copy-start(f32[512,256]{1,0:T(8,128)} %get-tuple-element.10) | copy-start | bytes 1572868
  98.3 1.1 %copy-start.2 = (f32[256,256]{1,0:T(8,128)S(1)}, f32[256,256]{1,0:T(8,128)}, u32[]{:S(2)}) copy-start(f32[256,256]{1,0:T(8,128)} %get-tuple-element.11) | copy-start | bytes 786436

commit v2 on v1

v2 whole, which is shorter than its diff:
```python
import functools
import math

import jax
import jax.numpy as jnp
from jax import lax
from jax.experimental import pallas as pl
from jax.experimental.pallas import tpu as pltpu
from jax.sharding import PartitionSpec as P

MESH = pl.DeviceIdType.MESH
F32 = jnp.float32
BF16 = jnp.bfloat16
LOG2E = math.log2(math.e)
norm_floor = 0.25
TILE = 256


def dot_nn(a, b):
    return lax.dot_general(a, b, (((1,), (0,)), ((), ())), preferred_element_type=F32)


def dot_nt(a, b):
    return lax.dot_general(a, b, (((1,), (1,)), ((), ())), preferred_element_type=F32)


def dot_tn(a, b):
    return lax.dot_general(a, b, (((0,), (0,)), ((), ())), preferred_element_type=F32)


def halves(block, factor):
    width = block.shape[-1]
    lane = lax.broadcasted_iota(jnp.int32, block.shape, 1)
    wide = block.astype(F32) * factor
    return (
        jnp.where(lane < width // 2, wide, 0.0).astype(BF16),
        jnp.where(lane < width // 2, 0.0, wide).astype(BF16),
    )


def kernel(
    n,
    tp_n,
    q_ref,
    k_ref,
    lat_ref,
    w_ref,
    log_ref,
    pair_ref,
    cot_ref,
    lam_ref,
    gain_ref,
    dq_ref,
    dk_ref,
    dv_ref,
    dw_ref,
    kbuf,
    vbuf,
    qbuf,
    gbuf,
    abuf,
    lbuf,
    own_v,
    own_g,
    own_a,
    col_a,
    own_k2,
    own_q2,
    part,
    wbuf,
    lat_send,
    lat_recv,
    fwd_send,
    fwd_recv,
    k_send,
    k_recv,
    v_send,
    v_recv,
    q_send,
    q_recv,
    g_send,
    g_recv,
    a_send,
    a_recv,
    w_send,
    w_recv,
):
    heads = lam_ref.shape[0]
    rows = q_ref.shape[0]
    width = q_ref.shape[1] // heads
    me = lax.axis_index("sp")
    tp = lax.axis_index("tp")
    chain = n // 2
    pos = me // 2
    col = me % 2
    factor = (width // 2) ** (-0.5)

    barrier = pltpu.get_barrier_semaphore()

    def greet_sp(i, carry):
        @pl.when(i != me)
        def _():
            pl.semaphore_signal(barrier, inc=1, device_id=(i, tp), device_id_type=MESH)

        return carry

    def greet_tp(i, carry):
        @pl.when(i != tp)
        def _():
            pl.semaphore_signal(barrier, inc=1, device_id=(me, i), device_id_type=MESH)

        return carry

    lax.fori_loop(0, n, greet_sp, 0)
    lax.fori_loop(0, tp_n, greet_tp, 0)
    pl.semaphore_wait(barrier, n - 1 + tp_n - 1)

    core = tp % 2
    pair = tp // 2
    mate = 2 * pair + 1 - core
    pairs = tp_n // 2

    def rc(src, dst, ssem, rsem, dev):
        return pltpu.make_async_remote_copy(
            src_ref=src,
            dst_ref=dst,
            send_sem=ssem,
            recv_sem=rsem,
            device_id=dev,
            device_id_type=MESH,
        )

    def lat_copy(slot_src, y):
        return rc(
            lat_ref, lbuf.at[slot_src], lat_send.at[y], lat_recv.at[slot_src], (me, 2 * y + core)
        )

    def lat_mate():
        return rc(lat_ref, lbuf.at[tp], fwd_send.at[tp], fwd_recv.at[tp], (me, mate))

    def lat_fwd(src):
        return rc(lbuf.at[src], lbuf.at[src], fwd_send.at[src], fwd_recv.at[src], (me, mate))

    class Stream:
        def __init__(self, own, buf, ssem, rsem, step):
            self.own, self.buf, self.ssem, self.rsem, self.step = own, buf, ssem, rsem, step

        def onward(self):
            nxt = pos + self.step
            return jnp.logical_and(nxt >= 0, nxt < chain)

        def copy(self, h, src, ref, way):
            dev = (jnp.clip(me + 2 * self.step, 0, n - 1), 2 * pos + 1 - col)[way]
            return rc(
                ref,
                self.buf.at[h, src],
                self.ssem.at[h, way, src],
                self.rsem.at[h, src],
                (dev, tp),
            )

        def send_own(self, h, act):
            @pl.when(self.onward())
            def _():
                getattr(self.copy(h, me, self.own(h), 0), act)()

            @pl.when(col == (0 if self.step == 1 else 1))
            def _():
                getattr(self.copy(h, me, self.own(h), 1), act)()

        def forward(self, h, src, act):
            getattr(self.copy(h, src, self.buf.at[h, src], 1), act)()

            @pl.when(self.onward())
            def _():
                getattr(self.copy(h, src, self.buf.at[h, src], 0), act)()

        def wait(self, h, src):
            self.copy(h, src, self.buf.at[h, src], 0).wait_recv()

    def lanes(h):
        return slice(h * width, (h + 1) * width)

    ks = Stream(lambda h: k_ref.at[:, lanes(h)], kbuf, k_send, k_recv, 1)
    vs = Stream(lambda h: own_v.at[:, lanes(h)], vbuf, v_send, v_recv, 1)
    qs = Stream(lambda h: q_ref.at[:, lanes(h)], qbuf, q_send, q_recv, -1)
    gs = Stream(lambda h: own_g.at[:, lanes(h)], gbuf, g_send, g_recv, -1)
    as_ = Stream(lambda h: own_a.at[h], abuf, a_send, a_recv, -1)

    for y in range(pairs):

        @pl.when(y != pair)
        def _():
            lat_copy(tp, y).start()

    lat_mate().start()
    qs.send_own(0, "start")
    ks.send_own(0, "start")

    lane = lax.broadcasted_iota(jnp.int32, (rows, 128), 1)
    packed = jnp.zeros((rows, 128), F32)
    log_rows = log_ref.shape[0]
    log_cols = jnp.transpose(
        jnp.concatenate([log_ref[...], jnp.zeros((128 - log_rows, rows), F32)], axis=0)
    )
    for h in range(heads):
        lam = lam_ref[h]
        a = pair_ref[:, (2 * h) * width : (2 * h + 1) * width].astype(F32)
        b = pair_ref[:, (2 * h + 1) * width : (2 * h + 2) * width].astype(F32)
        merged = a - lam * b
        inv = lax.rsqrt(jnp.mean(merged * merged, axis=-1, keepdims=True) + norm_floor)
        g = cot_ref[:, h * width : (h + 1) * width].astype(F32) * gain_ref[...]
        inner = jnp.mean(g * merged, axis=-1, keepdims=True)
        og = (inv * g - merged * (inv * inv * inv) * inner).astype(BF16)
        own_g[:, h * width : (h + 1) * width] = og
        wide = og.astype(F32)
        first = jnp.sum(wide * a, axis=-1, keepdims=True)
        second = jnp.sum(wide * b, axis=-1, keepdims=True)
        log_lam = jnp.log(jnp.full((1, 128), lam, F32))
        log0 = log_cols[:, 2 * h : 2 * h + 1] * LOG2E
        log1 = (log_cols[:, 2 * h + 1 : 2 * h + 2] - log_lam) * LOG2E
        packed = jnp.where(lane == 4 * h, log0, packed)
        packed = jnp.where(lane == 4 * h + 1, log1, packed)
        packed = jnp.where(lane == 4 * h + 2, first, packed)
        packed = jnp.where(lane == 4 * h + 3, second, packed)
    col_a[...] = packed
    flipped = jnp.transpose(packed)
    for h in range(heads):
        own_a[h, 0:4, :] = flipped[4 * h : 4 * h + 4, :]
        own_a[h, 4:8, :] = jnp.zeros((4, rows), F32)
    gs.send_own(0, "start")
    as_.send_own(0, "start")

    for h in range(heads):
        sl = slice(h * width, (h + 1) * width)
        k0, k1 = halves(k_ref[:, sl], factor)
        own_k2[0, :, sl] = k0
        own_k2[1, :, sl] = k1
        q0, q1 = halves(q_ref[:, sl], factor)
        own_q2[0, :, sl] = q0
        own_q2[1, :, sl] = q1

    def pass_down(h, s):
        src = 2 * (pos + s) + col

        @pl.when(pos + s < chain)
        def _():
            for stream in (qs, gs, as_):
                stream.wait(h, src)
                stream.forward(h, src, "start")

    def pass_keys(h, s):
        src = 2 * (pos - s) + col

        @pl.when(pos - s >= 0)
        def _():
            ks.wait(h, src)
            ks.forward(h, src, "start")

    pass_down(0, 1)
    pass_keys(0, 1)

    local = w_ref.shape[0] // tp_n

    def spread_latents():
        for y in range(pairs):

            @pl.when(y != pair)
            def _():
                src = 2 * y + core
                lat_copy(src, y).wait_recv()
                lat_fwd(src).start()

    def make_values():
        for y in range(pairs):
            lat_fwd(2 * y + 1 - core).wait_recv()
        lbuf[tp] = lat_ref[...]
        total = dot_nn(lbuf[0], w_ref[0:local, :])
        for i in range(1, tp_n):
            total += dot_nn(lbuf[i], w_ref[i * local : (i + 1) * local, :])
        own_v[...] = total.astype(BF16)
        vs.send_own(0, "start")

    def key_side(h, q_of, g_of, a_of, diagonal):
        sl = lanes(h)

        def tile(i, carry):
            ts = pl.ds(pl.multiple_of(i * TILE, TILE), TILE)
            q = q_of()
            g = g_of()
            q0, q1 = halves(q, factor)
            s0 = dot_nt(own_k2[0, ts, sl], q)
            s1 = dot_nt(own_k2[1, ts, sl], q)
            vd = dot_nt(own_v[ts, sl], g)
            p0 = jnp.exp2(s0 * LOG2E - a_of(0))
            p1 = jnp.exp2(s1 * LOG2E - a_of(1))
            if diagonal:
                spos = i * TILE + lax.broadcasted_iota(jnp.int32, (TILE, rows), 0)
                tpos = lax.broadcasted_iota(jnp.int32, (TILE, rows), 1)
                vis = spos <= tpos
                p0 = jnp.where(vis, p0, 0.0)
                p1 = jnp.where(vis, p1, 0.0)
            mixed = (p0 - p1).astype(BF16)
            d0 = (p0 * (vd - a_of(2))).astype(BF16)
            d1 = (p1 * (a_of(3) - vd)).astype(BF16)
            dvt = dot_nn(mixed, g)
            dkt = dot_nn(d0, q0) + dot_nn(d1, q1)
            if diagonal:
                dv_ref[ts, sl] = dvt
                dk_ref[ts, sl] = dkt
            else:
                dv_ref[ts, sl] += dvt
                dk_ref[ts, sl] += dkt
            return carry

        lax.fori_loop(0, rows // TILE, tile, 0)

    def query_side(h, k_of, v_of, diagonal):
        sl = lanes(h)

        def tile(i, carry):
            ts = pl.ds(pl.multiple_of(i * TILE, TILE), TILE)
            k = k_of()
            v = v_of()
            k0, k1 = halves(k, factor)
            s0 = dot_nt(own_q2[0, ts, sl], k)
            s1 = dot_nt(own_q2[1, ts, sl], k)
            vd = dot_nt(own_g[ts, sl], v)
            aux = col_a[ts, :]
            p0 = jnp.exp2(s0 * LOG2E - aux[:, 4 * h : 4 * h + 1])
            p1 = jnp.exp2(s1 * LOG2E - aux[:, 4 * h + 1 : 4 * h + 2])
            if diagonal:
                tpos = i * TILE + lax.broadcasted_iota(jnp.int32, (TILE, rows), 0)
                spos = lax.broadcasted_iota(jnp.int32, (TILE, rows), 1)
                vis = spos <= tpos
                p0 = jnp.where(vis, p0, 0.0)
                p1 = jnp.where(vis, p1, 0.0)
            d0 = (p0 * (vd - aux[:, 4 * h + 2 : 4 * h + 3])).astype(BF16)
            d1 = (p1 * (aux[:, 4 * h + 3 : 4 * h + 4] - vd)).astype(BF16)
            dqt = dot_nn(d0, k0) + dot_nn(d1, k1)
            if diagonal:
                dq_ref[ts, sl] = dqt
            else:
                dq_ref[ts, sl] += dqt
            return carry

        lax.fori_loop(0, rows // TILE, tile, 0)

    block = dw_ref.shape[0]

    def w_copy(h, dst):
        return rc(
            part.at[h, pl.ds(pl.multiple_of(dst * block, block), block)],
            wbuf.at[h, me],
            w_send.at[h, dst],
            w_recv.at[h, me],
            (dst, tp),
        )

    def w_wait(h, src):
        rc(
            part.at[h, pl.ds(0, block)],
            wbuf.at[h, src],
            w_send.at[h, src],
            w_recv.at[h, src],
            (src, tp),
        ).wait_recv()

    def weight_partials(h):
        per = local // block

        def one_slot(i, carry):
            slot = tp_n - 1 - i
            part[h, pl.ds(pl.multiple_of(slot * local, local), local), :] = dot_tn(
                lbuf[slot], dv_ref[:, lanes(h)].astype(BF16)
            ).astype(BF16)
            for r in range(per):
                dst = slot * per + per - 1 - r

                @pl.when(dst != me)
                def _():
                    w_copy(h, dst).start()

            return carry

        lax.fori_loop(0, tp_n, one_slot, 0)

    def key_slot(h, src):
        key_side(
            h,
            lambda: qbuf[h, src],
            lambda: gbuf[h, src],
            lambda r: abuf[h, src, r : r + 1, :],
            False,
        )

    def query_slot(h, src):
        query_side(h, lambda: kbuf[h, src], lambda: vbuf[h, src], False)

    def run_head(h):
        sl = lanes(h)
        more = h + 1 < heads
        lag = 2 if h == 0 else 0
        vlag = 2 if h == 0 else 1
        total_steps = chain + vlag + 1
        if h == 0 and more:
            total_steps = max(total_steps, 2 * chain - 1)

        def step(s, carry):
            if h == 0:

                @pl.when(s > 0)
                def _():
                    pass_down(h, s + 1)
                    pass_keys(h, s + 1)

                @pl.when(s == 1)
                def _():
                    spread_latents()

            if more:

                @pl.when(s == 0)
                def _():
                    for stream in (qs, gs, as_):
                        stream.send_own(h + 1, "start")

                @pl.when(s == pos)
                def _():
                    ks.send_own(h + 1, "start")

                @pl.when(s > chain - 1 - pos)
                def _():
                    pass_down(h + 1, s - (chain - 1 - pos))

                @pl.when(s > pos)
                def _():
                    pass_keys(h + 1, s - pos)

            if h == 0:

                @pl.when(s == 2)
                def _():
                    make_values()

            if more:

                @pl.when(s == jnp.maximum(pos, 2))
                def _():
                    vs.send_own(h + 1, "start")

            @pl.when(s == lag)
            def _():
                key_side(
                    h,
                    lambda: q_ref[:, sl],
                    lambda: own_g[:, sl],
                    lambda r: own_a[h, r : r + 1, :],
                    True,
                )

            up = s - vlag
            up_own = pos - up
            has_up = jnp.logical_and(up_own >= 0, up >= 1)

            @pl.when(has_up)
            def _():
                vs.wait(h, 2 * up_own + col)
                vs.forward(h, 2 * up_own + col, "start")

            far = s - lag
            down_side = 2 * (pos + far) + 1 - col
            side_down = jnp.logical_and(
                jnp.logical_and(pos + far < chain, far >= 0), jnp.logical_or(far > 0, col == 0)
            )

            @pl.when(jnp.logical_and(pos + far + 1 < chain, far >= 0))
            def _():
                key_slot(h, 2 * (pos + far + 1) + col)

            @pl.when(side_down)
            def _():
                for stream in (qs, gs, as_):
                    stream.wait(h, down_side)
                key_slot(h, down_side)

            @pl.when(far == chain - 1)
            def _():
                weight_partials(h)

            @pl.when(s == lag)
            def _():
                query_side(h, lambda: k_ref[:, sl], lambda: own_v[:, sl], True)

            @pl.when(has_up)
            def _():
                query_slot(h, 2 * up_own + col)

            side = up - 1
            up_side = 2 * (pos - side) + 1 - col
            side_up = jnp.logical_and(
                jnp.logical_and(pos - side >= 0, side >= 0), jnp.logical_or(side > 0, col == 1)
            )

            @pl.when(side_up)
            def _():
                ks.wait(h, up_side)
                vs.wait(h, up_side)
                query_slot(h, up_side)

            return carry

        lax.fori_loop(0, total_steps, step, 0)

    if heads > 2:
        raise NotImplementedError
    for h in range(heads):
        run_head(h)

    own_rows = pl.ds(pl.multiple_of(me * block, block), block)
    for h in range(heads):
        dw_ref[:, lanes(h)] = part[h, own_rows, :].astype(F32)

        def w_add(i, carry):
            src = (me + n - i) % n
            w_wait(h, src)
            dw_ref[:, lanes(h)] += wbuf[h, src].astype(F32)
            return carry

        lax.fori_loop(1, n, w_add, 0)

    for h in range(heads):

        def w_done(i, carry):
            w_copy(h, (me + i) % n).wait_send()
            return carry

        lax.fori_loop(1, n, w_done, 0)

        for stream in (qs, ks, gs, as_, vs):
            stream.send_own(h, "wait_send")

        def drain(s, carry):
            @pl.when(pos + s < chain)
            def _():
                for stream in (qs, gs, as_):
                    stream.forward(h, 2 * (pos + s) + col, "wait_send")

            @pl.when(pos - s >= 0)
            def _():
                for stream in (ks, vs):
                    stream.forward(h, 2 * (pos - s) + col, "wait_send")

            return carry

        lax.fori_loop(1, chain, drain, 0)

    lat_mate().wait_send()
    for y in range(pairs):

        @pl.when(y != pair)
        def _():
            lat_copy(tp, y).wait_send()
            lat_fwd(2 * y + core).wait_send()


def solution(mesh):
    n = mesh.shape["sp"]
    tp_n = mesh.shape["tp"]

    def step(q, k, lat, w, logs, pair, cot, lam, gain):
        rows, qcols = q.shape
        dmodel, vcols = w.shape
        block = dmodel // n
        heads = lam.shape[0]
        width = vcols // heads
        vmem = pl.BlockSpec(memory_space=pltpu.VMEM)
        dma = pltpu.SemaphoreType.DMA
        return pl.pallas_call(
            functools.partial(kernel, n, tp_n),
            name="diff_backward",
            out_shape=(
                jax.ShapeDtypeStruct((rows, qcols), F32),
                jax.ShapeDtypeStruct((rows, qcols), F32),
                jax.ShapeDtypeStruct((rows, vcols), F32),
                jax.ShapeDtypeStruct((block, vcols), F32),
            ),
            in_specs=[vmem] * 7 + [pl.BlockSpec(memory_space=pltpu.SMEM), vmem],
            out_specs=(vmem,) * 4,
            scratch_shapes=[
                pltpu.VMEM((heads, n, rows, width), BF16),
                pltpu.VMEM((heads, n, rows, width), BF16),
                pltpu.VMEM((heads, n, rows, width), BF16),
                pltpu.VMEM((heads, n, rows, width), BF16),
                pltpu.VMEM((heads, n, 8, rows), F32),
                pltpu.VMEM((tp_n,) + lat.shape, BF16),
                pltpu.VMEM((rows, vcols), BF16),
                pltpu.VMEM((rows, vcols), BF16),
                pltpu.VMEM((heads, 8, rows), F32),
                pltpu.VMEM((rows, 128), F32),
                pltpu.VMEM((2, rows, qcols), BF16),
                pltpu.VMEM((2, rows, qcols), BF16),
                pltpu.VMEM((heads, dmodel, width), BF16),
                pltpu.VMEM((heads, n, block, width), BF16),
                dma((tp_n // 2,)),
                dma((tp_n,)),
                dma((tp_n,)),
                dma((tp_n,)),
                dma((heads, 2, n)),
                dma((heads, n)),
                dma((heads, 2, n)),
                dma((heads, n)),
                dma((heads, 2, n)),
                dma((heads, n)),
                dma((heads, 2, n)),
                dma((heads, n)),
                dma((heads, 2, n)),
                dma((heads, n)),
                dma((heads, n)),
                dma((heads, n)),
            ],
            compiler_params=pltpu.CompilerParams(
                collective_id=0, has_side_effects=True, vmem_limit_bytes=60 * 1024 * 1024
            ),
        )(q, k, lat, w, logs.T, pair, cot, lam, gain.reshape(1, -1))

    return jax.shard_map(
        step,
        mesh=mesh,
        in_specs=(
            P("sp", "tp"),
            P("sp", "tp"),
            P("sp", "tp"),
            P(None, "tp"),
            P("sp", "tp"),
            P("sp", "tp"),
            P("sp", "tp"),
            P("tp"),
            P(),
        ),
        out_specs=(P("sp", "tp"), P("sp", "tp"), P("sp", "tp"), P("sp", "tp")),
        check_vma=False,
    )
```

time: 100 us -> 87.7 us (0.88)
  the two profiles are of different devices: /device:TPU:27 before, /device:TPU:0 now
where the time goes in v2:
time: 87.7 us; the launch traced here: 87.4 us
  Pallas kernels  81.8 us (93%)
  local copies, waits for them, and re-layouts  4.95 us (6%)
    pallas_call x1, Pallas kernels, step(): pl.pallas_call(functools.partial(kernel, n, tp_n), name='diff_backward',...  81.8 us
    unnamed x10, local copies, waits for them, and re-layouts  4.95 us

profile of v2, /device:TPU:0, one launch (start us, length us, event | category | flops | bytes accessed | tf_op | source)
XLA Modules:
  0.0 87.4 jit_solution(2243749666432770539)
XLA Ops:
  0.6 81.8 %diff_backward.1 = (f32[512,256]{1,0:T(8,128)}, f32[512,256]{1,0:T(8,128)}, f32[512,256]{1,0:T(8,128)}, f32[256,256]{1,0:T(8,128)}) custom-call(bf16[512,256]{1,0:T(8,128)(2,1)} %q_ref.1, bf16[512,256]{1,0:T(8,128)(2,1)} %k_ref.1, bf16[512,512]{1,0:T(8,128)(2,1)} %lat_ref.1, bf16[2048,256]{1,0:T(8,128)(2,1)} %w_ref.1, f32[4,512]{1,0:T(4,128)} %bitcast.2, ...), custom_call_target="tpu_custom_call" | custom-call | tf_op jit(solution)/shard_map/diff_backward/pallas_call | solution.py:579
  82.5 0.0 copy-start.1
  82.5 1.9 %copy.17 = f32[512,256]{1,0:T(8,128)} copy(f32[512,256]{1,0:T(8,128)} %get-tuple-element.8) | data formatting | bytes 1048576
  84.4 0.0 copy-done.1
  84.4 0.0 copy-start
  84.4 0.8 copy.18
  85.2 0.4 copy-done
  85.7 0.0 copy-start.2
  85.7 0.8 copy.19
  86.4 0.3 copy-done.2
  86.7 0.7 copy.20
Async XLA Ops:
  82.5 1.9 %copy-start.1 = (f32[512,256]{1,0:T(8,128)S(1)}, f32[512,256]{1,0:T(8,128)}, u32[]{:S(2)}) copy-start(f32[512,256]{1,0:T(8,128)} %get-tuple-element.9) | copy-start | bytes 1572868
  84.4 1.2 %copy-start = (f32[512,256]{1,0:T(8,128)S(1)}, f32[512,256]{1,0:T(8,128)}, u32[]{:S(2)}) copy-start(f32[512,256]{1,0:T(8,128)} %get-tuple-element.10) | copy-start | bytes 1572868
  85.7 1.1 %copy-start.2 = (f32[256,256]{1,0:T(8,128)S(1)}, f32[256,256]{1,0:T(8,128)}, u32[]{:S(2)}) copy-start(f32[256,256]{1,0:T(8,128)} %get-tuple-element.11) | copy-start | bytes 786436
